TPU v7x, 32 devices: a whole 2x2x4 slice. The times are simulated.
32 devices in a mesh: ep: 8 (over z, y), tp: 4 (over x, core).
Axes of the slice: x: 2, y: 2, z: 4, core: 2. Of those that a mesh axis runs over, the one named last changes fastest.
Arguments:
- queries: bfloat16 [4096, 2048], P('ep', 'tp'), may hold values from -6 to 6
- key_rows: bfloat16 [4096, 2048], P('ep', 'tp'), may hold values from -6 to 6
- value_rows: bfloat16 [4096, 4096], P('ep', 'tp'), may hold values from -6 to 6
- gate_rows: bfloat16 [4096, 4096], P('ep', 'tp'), may hold values from -6 to 6
- log_decay: float32 [16, 4096], P('tp', 'ep'), may hold values from -1 to 0
- head_gain: float32 [4096], P('tp'), may hold values from 0.1 to 1.9
- out_weight: bfloat16 [4096, 4096], P('tp'), may hold values from -0.09375 to 0.09375
- expert_input: bfloat16 [4096, 4096], P('ep'), may hold values from -6 to 6
- input_gain: float32 [4096], replicated, may hold values from 0.1 to 1.9
- route_ids: int32 [4096, 2], P('ep'), may hold values from 0 to 7, as said below
- route_weight: float32 [4096, 2], P('ep'), may hold values from 0.1 to 0.9
- expert_gate: bfloat16 [8, 4096, 1024], P('ep', None, 'tp'), may hold values from -0.09375 to 0.09375
- expert_up: bfloat16 [8, 4096, 1024], P('ep', None, 'tp'), may hold values from -0.09375 to 0.09375
- expert_down: bfloat16 [8, 1024, 4096], P('ep', 'tp'), may hold values from -0.1875 to 0.1875
Outputs:
- mixer_out: bfloat16 [4096, 4096], P(('ep', 'tp'))
- expert_out: bfloat16 [4096, 4096], P('ep', 'tp')
Inputs may be any that keep to these rules, and one draw needn't show every extreme that they name: `route_ids`: each row names two different experts of one group of 8 consecutive experts. On the rows of one device each group is named by exactly 512 rows, experts 2 i and 2 i + 1 together are named exactly 4 * 192 / 3 times, and no expert is named by more than 192 rows; one expert is named by exactly 192 rows of every device.
All inputs are finite; a program needn't handle non-finite values.
Results may differ from a plain program's by a relative error of at most 0.019.
Values may be sent and summed in bfloat16 or wider, within the bound.
A program may use at most 192 MiB of HBM per device.

v0:
```python
import jax
import jax.numpy as jnp
from jax import lax
from jax.sharding import PartitionSpec as P

BLOCK = 512
epsilon = 1e-06
theta_base = 10000.0
largest_entry = lax.Precision.HIGHEST


def prefix(value, axis, combine, identity):
    length, index = (lax.axis_size(axis), lax.axis_index(axis))
    everything = jax.tree.map(
        lambda part, kind: lax.all_gather(part.astype(kind), axis),
        value,
        (jnp.bfloat16, jnp.bfloat16),
    )
    start = jax.tree.map(
        lambda part, zero: jnp.broadcast_to(jnp.asarray(zero, part.dtype), part.shape),
        value,
        identity,
    )

    def hop(k, before):
        reached = k < index
        new = combine(
            before, jax.tree.map(lambda part, own: part[k].astype(own.dtype), everything, value)
        )
        return jax.tree.map(lambda a, b: jnp.where(reached, a, b), new, before)

    return lax.fori_loop(0, length, hop, start)


def rotate(values, positions):
    half_dim = values.shape[-1] // 2
    frequency = theta_base ** (-jnp.arange(half_dim, dtype=jnp.float32) / half_dim)
    angles = positions.astype(jnp.float32)[:, None, None] * frequency
    cosine = jnp.cos(angles)
    sine_wave = jnp.sin(angles)
    first_half = values[..., :half_dim]
    second = values[..., half_dim:]
    return jnp.concatenate(
        [first_half * cosine - second * sine_wave, second * cosine + first_half * sine_wave],
        axis=-1,
    )


def round_back(values):
    return lax.optimization_barrier(values.astype(jnp.bfloat16)).astype(jnp.float32)


def to_blocks(array, blocks):
    return array.reshape(blocks, array.shape[0] // blocks, array.shape[1], array.shape[2])


def combine_states(earlier, later):
    return (later[1][:, None, None] * earlier[0] + later[0], earlier[1] * later[1])


def retention_rows(queries, key_rows, value_rows, gate_rows, log_decay, head_gain):
    length = queries.shape[0]
    head_count = log_decay.shape[0]
    key_width = queries.shape[1] // head_count
    value_width = value_rows.shape[1] // head_count
    blocks = length // BLOCK
    positions = lax.axis_index("ep") * length + jnp.arange(length, dtype=jnp.int32)
    query_rot = to_blocks(
        rotate(queries.astype(jnp.float32).reshape(length, head_count, key_width), positions),
        blocks,
    )
    key_rot = to_blocks(
        rotate(key_rows.astype(jnp.float32).reshape(length, head_count, key_width), positions)
        * key_width ** (-0.5),
        blocks,
    )
    value_all = to_blocks(
        value_rows.astype(jnp.float32).reshape(length, head_count, value_width), blocks
    )
    running = jnp.cumsum(log_decay.reshape(head_count, blocks, BLOCK), axis=2)
    ending = running[:, :, -1]
    kept = jnp.exp(ending[:, :, None] - running)
    block_states = jnp.einsum(
        "nlhd,hnl,nlhe->nhde", key_rot, kept, value_all, precision=largest_entry
    )
    block_decay = jnp.exp(ending).T

    def advance(carried, inputs):
        decay_now, state_now = inputs
        return (decay_now[:, None, None] * carried + state_now, carried)

    zeros_state = jnp.zeros((head_count, key_width, value_width), jnp.float32)
    device_state, local_starts = lax.scan(advance, zeros_state, (block_decay, block_states))
    device_decay = jnp.exp(jnp.sum(ending, axis=1))
    incoming, passed_decay = prefix(
        (device_state, device_decay),
        "ep",
        combine_states,
        (zeros_state, jnp.ones((head_count,), jnp.float32)),
    )
    causal = jnp.arange(BLOCK)[:, None] >= jnp.arange(BLOCK)[None, :]
    spread = running[:, :, :, None] - running[:, :, None, :]
    weight_table = jnp.exp(jnp.where(causal, spread, -jnp.inf))
    score_matrix = (
        jnp.einsum("nlhd,nmhd->hnlm", query_rot, key_rot, precision=largest_entry) * weight_table
    )
    inside = jnp.einsum("hnlm,nmhe->nlhe", score_matrix, value_all, precision=largest_entry)
    before = jnp.exp(jnp.cumsum(ending, axis=1) - ending)
    starts = local_starts + before.T[:, :, None, None] * incoming[None]
    outside = jnp.einsum(
        "nlhd,hnl,nhde->nlhe", query_rot, jnp.exp(running), starts, precision=largest_entry
    )
    mixed = (inside + outside).reshape(length, head_count, value_width)
    centered = mixed - jnp.mean(mixed, axis=-1, keepdims=True)
    normed = (
        centered
        * lax.rsqrt(jnp.mean(centered * centered, axis=-1, keepdims=True) + epsilon)
        * head_gain.reshape(head_count, value_width)
    )
    return (
        jax.nn.silu(gate_rows.astype(jnp.float32))
        * normed.reshape(length, head_count * value_width)
    ).astype(jnp.bfloat16)


def body(
    queries,
    key_rows,
    value_rows,
    gate_rows,
    log_decay,
    head_gain,
    out_weight,
    expert_input,
    input_gain,
    route_ids,
    route_weight,
    expert_gate,
    expert_up,
    expert_down,
):
    hidden = retention_rows(queries, key_rows, value_rows, gate_rows, log_decay, head_gain)
    tp_count = lax.axis_size("tp")
    model_width = out_weight.shape[1]
    mixer_out = lax.psum_scatter(
        jnp.dot(hidden, out_weight, preferred_element_type=jnp.float32).astype(jnp.bfloat16),
        "tp",
        scatter_dimension=0,
        tiled=True,
    )
    token_count = expert_input.shape[0]
    local_experts = expert_gate.shape[0]
    ep_count = lax.axis_size("ep")
    expert_count = ep_count * local_experts
    capacity = 3 * token_count // expert_count
    quarter = model_width // tp_count
    widened = expert_input.astype(jnp.float32)
    normed = (
        widened
        * lax.rsqrt(jnp.mean(widened * widened, axis=-1, keepdims=True) + epsilon)
        * input_gain
    ).astype(jnp.bfloat16)
    flat_ids = route_ids.reshape(-1)
    matches = (flat_ids[:, None] == jnp.arange(expert_count, dtype=jnp.int32)[None, :]).astype(
        jnp.int32
    )
    slot_rank = jnp.sum((jnp.cumsum(matches, axis=0) - matches) * matches, axis=1)
    target = flat_ids * capacity + slot_rank
    owners = jnp.arange(2 * token_count, dtype=jnp.int32) // 2
    slot_table = jnp.full((expert_count * capacity,), token_count, jnp.int32).at[target].set(owners)
    padded = jnp.concatenate([normed, jnp.zeros((1, model_width), jnp.bfloat16)], axis=0)
    share = capacity // tp_count
    own_slots = lax.dynamic_slice_in_dim(
        slot_table.reshape(expert_count, capacity), lax.axis_index("tp") * share, share, 1
    )
    outgoing = padded[own_slots]
    arrived = lax.all_to_all(outgoing, "ep", split_axis=0, concat_axis=0, tiled=True).reshape(
        ep_count, local_experts, share, model_width
    )
    gate_whole, up_whole, down_whole = (
        lax.all_gather(expert_gate, "tp", axis=2, tiled=True),
        lax.all_gather(expert_up, "tp", axis=2, tiled=True),
        lax.all_gather(expert_down, "tp", axis=1, tiled=True),
    )
    gate_val = jnp.einsum("sxcd,xdf->sxcf", arrived, gate_whole, preferred_element_type=jnp.float32)
    up_val = jnp.einsum("sxcd,xdf->sxcf", arrived, up_whole, preferred_element_type=jnp.float32)
    inner_rows = (jax.nn.silu(gate_val) * up_val).astype(jnp.bfloat16)
    unit_group = expert_down.shape[1]
    group_parts = jnp.einsum(
        "sxcgf,xgfd->gsxcd",
        inner_rows.reshape(ep_count, local_experts, share, tp_count, unit_group),
        down_whole.reshape(local_experts, tp_count, unit_group, model_width),
        preferred_element_type=jnp.float32,
    )
    finished = jnp.sum(round_back(group_parts), axis=0).astype(jnp.bfloat16)
    came_back = lax.all_to_all(finished, "ep", split_axis=0, concat_axis=0, tiled=True)
    returned = lax.all_to_all(came_back, "tp", split_axis=3, concat_axis=2, tiled=True).reshape(
        expert_count * capacity, quarter
    )
    picked = returned[target].reshape(token_count, 2, quarter).astype(jnp.float32)
    expert_out = jnp.sum(picked * route_weight[:, :, None], axis=1).astype(jnp.bfloat16)
    return (mixer_out, expert_out)


def solution(mesh):
    placed = (
        P("ep", "tp"),
        P("ep", "tp"),
        P("ep", "tp"),
        P("ep", "tp"),
        P("tp", "ep"),
        P("tp"),
        P("tp", None),
        P("ep", None),
        P(),
        P("ep", None),
        P("ep", None),
        P("ep", None, "tp"),
        P("ep", None, "tp"),
        P("ep", "tp", None),
    )
    return jax.shard_map(
        body,
        mesh=mesh,
        in_specs=placed,
        out_specs=(P(("ep", "tp"), None), P("ep", "tp")),
        check_vma=False,
    )
```

profile of v0, /device:TPU:0, one launch (start us, length us, event | category | flops | bytes accessed | tf_op | source)
XLA Modules:
  0.0 503.5 jit_solution(17845343262958947994)
XLA Ops:
  31.4 4.8 scatter_custom_fusion
  45.3 11.0 %gather_fusion = bf16[384,4096]{1,0:T(8,128)(2,1)} fusion(bf16[513,4096]{1,0:T(8,128)(2,1)} %concatenate.14, s32[1024]{0:T(1024)S(1)} %pad_clamp_fusion), kind=kCustom, calls=%fused_computation | custom fusion | bytes 6292992 | tf_op jit(solution)/shard_map/gather | solution.py:176
  56.6 7.2 %all-to-all-start = ((bf16[8,48,4096]{2,1,0:T(8,128)(2,1)}), bf16[8,48,4096]{2,1,0:T(8,128)(2,1)}, u32[]{:S(2)}, u32[]{:S(2)}) async-start(bf16[8,48,4096]{2,1,0:T(8,128)(2,1)} %bitcast.27), calls=%async_computation.1 | async-start | bytes 6291456 | tf_op jit(solution)/shard_map/all_to_all | solution.py:177
  63.8 74.4 %all-reduce.1 = bf16[32]{0:T(256)(128)(2,1)S(1)} all-reduce(bf16[32]{0:T(256)(128)(2,1)S(1)} %dynamic-update-slice), channel_id=2, replica_groups=mesh['ep'=8,'tp'=4] {'ep'}, use_global_device_ids=true, to_apply=%add.1 | all-reduce | flops 32 | bytes 128
  138.5 5.4 %fusion.50 = f32[4,512,512]{2,1,0:T(8,128)S(1)} fusion(f32[512,4,64]{2,0,1:T(8,128)} %get-tuple-element.148, f32[512,4,64]{2,0,1:T(8,128)} %get-tuple-element.149, f32[512,4,64]{2,0,1:T(8,128)S(1)} %get-tuple-element.145, f32[512,4,64]{2,0,1:T(8,128)S(1)} %get-tuple-element.144), kind=kOutput, calls=%fused_computation.70 | convolution fusion | flops 1611399168 | bytes 6291456 | tf_op jit(solution)/shard_map/nlhd,nmhd->hnlm/dot_general | solution.py:105
  143.9 4.6 fusion.8
  148.5 9.1 %while.9 = (s32[]{:T(128)}, f32[4,128,256]{2,1,0:T(8,128)S(1)}, s32[]{:T(128)}, bf16[8,4]{1,0:T(8,128)(2,1)S(1)}, bf16[8,4,128,256]{3,2,1,0:T(8,128)(2,1)}, /*index=5*/s32[]{:T(128)}, s32[]{:T(128)}) while((s32[]{:T(128)}, f32[4,128,256]{2,1,0:T(8,128)S(1)}, s32[]{:T(128)}, bf16[8,4]{1,0:T(8,128)(2,1)S(1)}, ...), condition=%wide.region_3.4_spmd.clone, body=%wide.region_2.3_spmd.clone.sunk | while | flops 655368 | bytes 1310865 | solution.py:32
  157.6 4.9 fusion.71
  171.8 12.7 %convolution_convert_fusion = bf16[512,4096]{1,0:T(8,128)(2,1)} fusion(bf16[1024,4096]{1,0:T(8,128)(2,1)} %param.22, f32[512,1024]{1,0:T(8,128)} %bitcast.162, f32[512,1024]{1,0:T(8,128)} %copy.83, f32[512,1024]{1,0:T(8,128)} %copy.84, bf16[512,1024]{1,0:T(8,128)(2,1)} %param.19, f32[1024]{0:T(1024)S(1)} %copy-done.7), kind=kOutput, calls=%fused_computation.16 | convolution fusion | flops 4302307328 | bytes 19927040 | tf_op jit(solution)/shard_map/dot_general | solution.py:146
  184.6 7.2 %fusion.6 = f32[8,48,1024]{2,1,0:T(8,128)S(1)} fusion(bf16[8,48,4096]{2,1,0:T(8,128)(2,1)} %all-to-all-done, bf16[1,4096,1024]{2,1,0:T(8,128)(2,1)} %all-gather.7.cloned.1.call-done), kind=kOutput, calls=%fused_computation.14 | convolution fusion | flops 3221225472 | bytes 13107200 | tf_op jit(solution)/shard_map/sxcd,xdf->sxcf/dot_general | solution.py:185
  191.8 41.9 %all-gather.9.cloned.1.call-done = bf16[1,4096,1024]{2,1,0:T(8,128)(2,1)} async-done(((bf16[1,4096,256]{2,1,0:T(8,128)(2,1)}), bf16[1,4096,1024]{2,1,0:T(8,128)(2,1)}) %all-gather.9.cloned.1.call-update) | async-done | bytes 8388624 | tf_op jit(solution)/shard_map/all_gather | solution.py:182
  233.6 7.9 %fusion.27 = bf16[8,1,48,1024]{3,2,0,1:T(8,128)(2,1)S(1)} fusion(f32[8,48,1024]{2,1,0:T(8,128)S(1)} %fusion.6, bf16[8,48,4096]{2,1,0:T(8,128)(2,1)} %all-to-all-done, bf16[1,4096,1024]{2,1,0:T(8,128)(2,1)} %all-gather.9.cloned.1.call-done), kind=kOutput, calls=%fused_computation.42 | convolution fusion | flops 3223584768 | bytes 13893632 | tf_op jit(solution)/shard_map/sxcd,xdf->sxcf/dot_general | solution.py:186
  242.1 51.3 %all-gather.11.cloned.1.call-done = bf16[1,1024,4096]{2,1,0:T(8,128)(2,1)} async-done(((bf16[1,256,4096]{2,1,0:T(8,128)(2,1)}), bf16[1,1024,4096]{2,1,0:T(8,128)(2,1)}) %all-gather.11.cloned.1.call-update) | async-done | bytes 8388624 | tf_op jit(solution)/shard_map/all_gather | solution.py:183
  293.3 10.3 %convert_bitcast_fusion = bf16[4,8,1,48,4096]{4,3,1,0,2:T(8,128)(2,1)} fusion(bf16[4,256,4096,1]{2,1,3,0:T(8,128)(2,1)} %bitcast.159, bf16[8,48,4,256]{3,2,1,0:T(4,128)(2,1)S(1)} %reshape.414), kind=kOutput, calls=%fused_computation.6 | convolution fusion | flops 3227516928 | bytes 21757952 | tf_op jit(solution)/shard_map/sxcgf,xgfd->gsxcd/dot_general | solution.py:189
  303.6 8.6 %reduce_sum.70 = bf16[8,48,4096]{2,1,0:T(8,128)(2,1)S(1)} reduce(bf16[4,8,1,48,4096]{4,3,1,0,2:T(8,128)(2,1)} %convert_bitcast_fusion, bf16[]{:T(256)} %constant.105.clone.1), dimensions={0,2}, to_apply=%region_12.13 | reduce | flops 4718592 | bytes 15728642 | tf_op jit(solution)/shard_map/reduce_sum | solution.py:195
  312.2 76.6 %all_to_all.25 = bf16[8,1,48,4096]{3,2,1,0:T(8,128)(2,1)} all-to-all(bf16[8,1,48,4096]{3,2,1,0:T(8,128)(2,1)S(1)} %bitcast.155), channel_id=1, replica_groups=mesh['ep'=8,'tp'=4] {'ep'}, dimensions={0} | all-to-all | bytes 6291456 | tf_op jit(solution)/shard_map/all_to_all | solution.py:196
  388.8 9.7 %copy.90 = bf16[8,1,48,4096]{2,0,1,3:T(8,128)(2,1)} copy(bf16[8,1,48,4096]{3,2,1,0:T(8,128)(2,1)} %all_to_all.25) | data formatting | bytes 6291456 | tf_op jit(solution)/shard_map/all_to_all | solution.py:196
  398.5 14.8 %reshape.467 = bf16[4,2,196608]{2,1,0:T(2,128)(2,1)} reshape(bf16[4096,1,8,48]{3,2,1,0:T(8,128)(2,1)} %bitcast.152) | data formatting | bytes 6291456
  417.5 36.7 %all-to-all-done.2 = bf16[4,2,196608]{2,1,0:T(2,128)(2,1)S(1)} async-done(((bf16[4,2,196608]{2,1,0:T(2,128)(2,1)}), bf16[4,2,196608]{2,1,0:T(2,128)(2,1)S(1)}, u32[]{:S(2)}, u32[]{:S(2)}) %all-to-all-start.2) | async-done | bytes 3145760 | tf_op jit(solution)/shard_map/all_to_all | solution.py:197
  454.2 9.9 %reshape.468 = bf16[4096,1,8,48]{3,2,1,0:T(8,128)(2,1)} reshape(bf16[4,2,196608]{2,1,0:T(2,128)(2,1)S(1)} %all-to-all-done.2) | data formatting | bytes 6291456
  464.1 10.2 %copy.99 = bf16[8,1,48,4,1024]{4,3,2,0,1:T(4,128)(2,1)} copy(bf16[8,1,48,4,1024]{2,0,4,3,1:T(8,128)(2,1)} %bitcast.153) | data formatting | bytes 6291456 | tf_op jit(solution)/shard_map/all_to_all | solution.py:197
  477.3 5.4 %gather_fusion.1 = bf16[1024,1024]{1,0:T(8,128)(2,1)} fusion(bf16[1536,1024]{1,0:T(8,128)(2,1)S(1)} %bitcast.151, s32[1024]{0:T(1024)S(1)} %broadcast_clamp_fusion), kind=kCustom, calls=%fused_computation.1 | custom fusion | bytes 4198400 | tf_op jit(solution)/shard_map/gather | solution.py:200
  482.7 5.4 %reshape.423 = f32[512,2,1024]{2,1,0:T(2,128)} reshape(bf16[1024,1024]{1,0:T(8,128)(2,1)} %gather_fusion.1) | data formatting | bytes 6291456 | tf_op jit(solution)/shard_map/convert_element_type | solution.py:200
  488.2 8.6 %multiply_reduce_fusion = bf16[512,1024]{1,0:T(8,128)(2,1)} fusion(f32[512,2,1024]{2,1,0:T(2,128)} %reshape.423, f32[512,2]{1,0:T(8,128)S(1)} %copy.93), kind=kLoop, calls=%fused_computation.17 | loop fusion | flops 1572864 | bytes 5246976 | tf_op jit(solution)/shard_map/reduce_sum | solution.py:201
  (116 shorter events, 58.4 us)
Async XLA Ops:
  7.2 141.3 %all-gather.13.cloned.1.call-start = ((), (), s32[]{:S(2)}) async-start(), calls=%async_computation.8 | async-start | bytes 2359296 | tf_op jit(solution)/shard_map/all_gather | solution.py:15
  9.5 4.2 copy-start.3
  18.2 4.1 copy-start.1
  25.5 2.1 copy-start.5
  25.5 159.0 %all-gather.7.cloned.1.call-start = ((), (), s32[]{:S(2)}) async-start(), calls=%async_computation.5 | async-start | bytes 10485760 | tf_op jit(solution)/shard_map/all_gather | solution.py:181
  26.3 10.1 %copy-start.8 = (u32[32]{0:T(128)S(1)}, u32[32]{0:T(128)}, u32[]{:S(2)}) copy-start(u32[32]{0:T(128)} %constant.120) | copy-start | bytes 388
  26.3 207.3 %all-gather.9.cloned.1.call-start = ((), (), s32[]{:S(2)}) async-start(), calls=%async_computation.6 | async-start | bytes 10485760 | tf_op jit(solution)/shard_map/all_gather | solution.py:182
  27.0 266.3 %all-gather.11.cloned.1.call-start = ((), (), s32[]{:S(2)}) async-start(), calls=%async_computation.7 | async-start | bytes 10485760 | tf_op jit(solution)/shard_map/all_gather | solution.py:183
  27.6 13.5 %copy-start.4 = (f32[4096]{0:T(1024)S(1)}, f32[4096]{0:T(1024)}, u32[]{:S(2)}) copy-start(f32[4096]{0:T(1024)} %param.24) | copy-start | bytes 49156
  36.4 4.7 copy-start
  56.6 128.0 %all-to-all-start = ((bf16[8,48,4096]{2,1,0:T(8,128)(2,1)}), bf16[8,48,4096]{2,1,0:T(8,128)(2,1)}, u32[]{:S(2)}, u32[]{:S(2)}) async-start(bf16[8,48,4096]{2,1,0:T(8,128)(2,1)} %bitcast.27), calls=%async_computation.1 | async-start | bytes 6291456 | tf_op jit(solution)/shard_map/all_to_all | solution.py:177
  63.8 433.0 %reduce-scatter.2.cloned.1.call-start = ((), (), s32[]{:S(2)}) async-start(), calls=%async_computation.4 | async-start | bytes 5242880 | tf_op jit(solution)/shard_map/reduce_scatter | solution.py:145
  138.5 5.5 %copy-start.2 = (bf16[512,1024]{1,0:T(8,128)(2,1)S(1)}, bf16[512,1024]{1,0:T(8,128)(2,1)}, u32[]{:S(2)}) copy-start(bf16[512,1024]{1,0:T(8,128)(2,1)} %param.18) | copy-start | bytes 3145732
  169.8 2.0 copy-start.7
  413.3 4.0 copy-start.6
  413.3 40.9 %all-to-all-start.2 = ((bf16[4,2,196608]{2,1,0:T(2,128)(2,1)}), bf16[4,2,196608]{2,1,0:T(2,128)(2,1)S(1)}, u32[]{:S(2)}, u32[]{:S(2)}) async-start(bf16[4,2,196608]{2,1,0:T(2,128)(2,1)} %reshape.467), calls=%async_computation.3 | async-start | bytes 6291456 | tf_op jit(solution)/shard_map/all_to_all | solution.py:197
Sparse Core Ops, SparseCore 0:
  25.7 72.0 all-gather.12
  99.3 73.3 all-gather.6
  174.2 59.3 all-gather.8
  235.0 58.2 all-gather.10
  296.3 44.5 reduce-scatter.1
where the time goes:
time: 511 us; the launch traced here: 503 us
  blocking collectives  151 us (30%)
  waiting for transfers between devices  132 us (26%)
  local copies, waits for them, and re-layouts  97.1 us (19%)
  matrix products  56.1 us (11%)
  other arithmetic  40.3 us (8%)
  between operations  15.4 us (3%)
  starting transfers between devices  11.4 us (2%)
    all_to_all x1, blocking collectives, body(): lax.all_to_all(finished, 'ep', split_axis=0, concat_axis=0, tiled=True)  76.6 us
    unnamed x1, blocking collectives  74.4 us
    all_gather x1, waiting for transfers between devices, body(): lax.all_gather(expert_down, 'tp', axis=1, tiled=True)  51.3 us
    all_gather x1, waiting for transfers between devices, body(): lax.all_gather(expert_up, 'tp', axis=2, tiled=True)  41.9 us
    all_to_all x1, waiting for transfers between devices, body(): lax.all_to_all(came_back, 'tp', split_axis=3, concat_axis=2, tiled=True)  36.7 us
    unnamed x32, local copies, waits for them, and re-layouts  34.6 us
    all_to_all x2, local copies, waits for them, and re-layouts, body(): lax.all_to_all(came_back, 'tp', split_axis=3, concat_axis=2, tiled=True)  13.2 us
    dot_general x1, matrix products, body(): jnp.dot(hidden, out_weight, preferred_element_type=jnp.float32)  12.7 us
  transfers between devices with their start and end apart: 7, of which 3 were waited for; matrix products, arithmetic and copies ran while one was open for 35% of the time, Pallas kernels for 0%

commit v1 on v0

--- a/solution.py
+++ b/solution.py
@@ -194,9 +194,10 @@
     )
     finished = jnp.sum(round_back(group_parts), axis=0).astype(jnp.bfloat16)
     came_back = lax.all_to_all(finished, "ep", split_axis=0, concat_axis=0, tiled=True)
-    returned = lax.all_to_all(came_back, "tp", split_axis=3, concat_axis=2, tiled=True).reshape(
-        expert_count * capacity, quarter
-    )
+    returned = jnp.concatenate(
+        lax.all_to_all(jnp.stack(jnp.split(came_back, lax.axis_size("tp"), axis=3)), "tp", 0, 0),
+        axis=2,
+    ).reshape(expert_count * capacity, quarter)
     picked = returned[target].reshape(token_count, 2, quarter).astype(jnp.float32)
     expert_out = jnp.sum(picked * route_weight[:, :, None], axis=1).astype(jnp.bfloat16)
     return (mixer_out, expert_out)

time: 511 us -> 471 us (0.922)
  blocking collectives: 151 us -> 74.5 us
  waiting for transfers between devices: 132 us -> 204 us
  local copies, waits for them, and re-layouts: 97.1 us -> 53.8 us
  starting transfers between devices: 11.4 us -> 17.3 us
    all_to_all x1 -> x0, blocking collectives: 76.6 us -> none  [body(): lax.all_to_all(finished, 'ep', split_axis=0, concat_axis=0, tiled=True)]
    all_to_all x1 -> x2, waiting for transfers between devices: 36.7 us -> 95.2 us  [the longest x1 58.5 us: body(): lax.all_to_all(finished, 'ep', split_axis=0, concat_axis=0, tiled=True)]
    all_to_all x3 -> x0, local copies, waits for them, and re-layouts: 22.9 us -> none  [the longest x2 13.2 us: body(): lax.all_to_all(came_back, 'tp', split_axis=3, concat_axis=2, tiled=True)]
    unnamed x32, local copies, waits for them, and re-layouts: 34.6 us -> 11.8 us
    all_gather x1, waiting for transfers between devices: 41.9 us -> 54 us  [body(): lax.all_gather(expert_up, 'tp', axis=2, tiled=True)]
    all_to_all x1 -> x2, starting transfers between devices: 4 us -> 9.48 us  [the longest x1 5.65 us: body(): lax.all_to_all(finished, 'ep', split_axis=0, concat_axis=0, tiled=True)]
  transfers between devices with their start and end apart: 7 -> 8, of which waited for: 3 -> 5; matrix products, arithmetic and copies ran while one was open for 35% -> 24% of each run, Pallas kernels for 0% -> 0%
where the time goes in v1:
time: 471 us; the launch traced here: 464 us
  waiting for transfers between devices  204 us (43%)
  blocking collectives  74.5 us (16%)
  matrix products  55.1 us (12%)
  local copies, waits for them, and re-layouts  53.8 us (11%)
  other arithmetic  43.6 us (9%)
  starting transfers between devices  17.3 us (4%)
  between operations  15.2 us (3%)
    unnamed x1, blocking collectives  74.5 us
    all_to_all x1, waiting for transfers between devices, body(): lax.all_to_all(finished, 'ep', split_axis=0, concat_axis=0, tiled=True)  58.5 us
    all_gather x1, waiting for transfers between devices, body(): lax.all_gather(expert_up, 'tp', axis=2, tiled=True)  54 us
    all_gather x1, waiting for transfers between devices, body(): lax.all_gather(expert_down, 'tp', axis=1, tiled=True)  51.1 us
    all_to_all x1, waiting for transfers between devices, body(): lax.all_to_all(jnp.stack(jnp.split(came_back, lax.axis_size('tp'), axis=3...  36.7 us
    dot_general x1, matrix products, body(): jnp.dot(hidden, out_weight, preferred_element_type=jnp.float32)  12.3 us
    unnamed x32, local copies, waits for them, and re-layouts  11.8 us
    gather x1, local copies, waits for them, and re-layouts, body(): outgoing = padded[own_slots]  11 us
  transfers between devices with their start and end apart: 8, of which 5 were waited for; matrix products, arithmetic and copies ran while one was open for 24% of the time, Pallas kernels for 0%

profile of v1, /device:TPU:0, one launch (start us, length us, event | category | flops | bytes accessed | tf_op | source)
XLA Modules:
  0.0 463.6 jit_solution(15630380015831466625)
XLA Ops:
  18.2 4.1 multiply_subtract_fusion
  31.3 4.8 %scatter_custom_fusion = s32[1536]{0:T(1024)S(1)} fusion(s32[1024]{0:T(1024)S(1)} %bitcast.179, s32[1024]{0:T(1024)S(1)} %add_select_fusion, s32[]{:T(128)} %constant.95.clone.1), kind=kCustom, calls=%fused_computation.99 | custom fusion | bytes 6148 | tf_op jit(solution)/shard_map/scatter | solution.py:170
  36.4 3.3 fusion.1
  44.0 11.0 %gather_fusion = bf16[384,4096]{1,0:T(8,128)(2,1)} fusion(bf16[513,4096]{1,0:T(8,128)(2,1)} %concatenate.14, s32[1024]{0:T(1024)S(1)} %pad_clamp_fusion), kind=kCustom, calls=%fused_computation | custom fusion | bytes 6292992 | tf_op jit(solution)/shard_map/gather | solution.py:176
  55.0 7.4 %all-to-all-start = ((bf16[8,48,4096]{2,1,0:T(8,128)(2,1)}), bf16[8,48,4096]{2,1,0:T(8,128)(2,1)}, u32[]{:S(2)}, u32[]{:S(2)}) async-start(bf16[8,48,4096]{2,1,0:T(8,128)(2,1)} %bitcast.27), calls=%async_computation.1 | async-start | bytes 6291456 | tf_op jit(solution)/shard_map/all_to_all | solution.py:177
  63.9 74.5 %all-reduce.1 = bf16[32]{0:T(256)(128)(2,1)S(1)} all-reduce(bf16[32]{0:T(256)(128)(2,1)S(1)} %dynamic-update-slice), channel_id=2, replica_groups=mesh['ep'=8,'tp'=4] {'ep'}, use_global_device_ids=true, to_apply=%add.1 | all-reduce | flops 32 | bytes 128
  138.6 5.4 %fusion.50 = f32[4,512,512]{2,1,0:T(8,128)S(1)} fusion(f32[512,4,64]{2,0,1:T(8,128)} %get-tuple-element.151, f32[512,4,64]{2,0,1:T(8,128)} %get-tuple-element.152, f32[512,4,64]{2,0,1:T(8,128)S(1)} %get-tuple-element.148, f32[512,4,64]{2,0,1:T(8,128)S(1)} %get-tuple-element.147), kind=kOutput, calls=%fused_computation.75 | convolution fusion | flops 1611399168 | bytes 6291456 | tf_op jit(solution)/shard_map/nlhd,nmhd->hnlm/dot_general | solution.py:105
  144.0 4.6 fusion.8
  148.6 9.1 %while.9 = (s32[]{:T(128)}, f32[4,128,256]{2,1,0:T(8,128)S(1)}, s32[]{:T(128)}, bf16[8,4]{1,0:T(8,128)(2,1)S(1)}, bf16[8,4,128,256]{3,2,1,0:T(8,128)(2,1)}, /*index=5*/s32[]{:T(128)}, s32[]{:T(128)}) while((s32[]{:T(128)}, f32[4,128,256]{2,1,0:T(8,128)S(1)}, s32[]{:T(128)}, bf16[8,4]{1,0:T(8,128)(2,1)S(1)}, ...), condition=%wide.region_3.4_spmd.clone, body=%wide.region_2.3_spmd.clone.sunk | while | flops 655368 | bytes 1310865 | solution.py:32
  157.6 4.9 %fusion.71 = (f32[512,4]{0,1:T(4,128)S(1)}, f32[1,512,4,256]{1,3,2,0:T(8,128)S(1)}) fusion(f32[4,128,256]{2,1,0:T(8,128)S(1)} %get-tuple-element.111, f32[4]{0:T(128)S(1)} %get-tuple-element.140, f32[4,512]{1,0:T(4,128)S(1)} %get-tuple-element.142, f32[512,4,64]{2,0,1:T(8,128)} %get-tuple-element.151, f32[512,4,64]{2,0,1:T(8,128)} %get-tuple-element.152, ...), kind=kOutput, calls=%fused_computation.123 | convolution fusion | flops 807008256 | bytes 5783568 | tf_op jit(solution)/shard_map/nlhd,hnl,nhde->nlhe/dot_general | solution.py:110
  173.4 7.0 %fusion.6 = f32[8,48,1024]{2,1,0:T(8,128)S(1)} fusion(bf16[8,48,4096]{2,1,0:T(8,128)(2,1)} %all-to-all-done, bf16[1,4096,1024]{2,1,0:T(8,128)(2,1)} %all-gather.7.cloned.1.call-done), kind=kOutput, calls=%fused_computation.14 | convolution fusion | flops 3221225472 | bytes 13107200 | tf_op jit(solution)/shard_map/sxcd,xdf->sxcf/dot_general | solution.py:185
  180.4 54.0 %all-gather.9.cloned.1.call-done = bf16[1,4096,1024]{2,1,0:T(8,128)(2,1)} async-done(((bf16[1,4096,256]{2,1,0:T(8,128)(2,1)}), bf16[1,4096,1024]{2,1,0:T(8,128)(2,1)}) %all-gather.9.cloned.1.call-update) | async-done | bytes 8388624 | tf_op jit(solution)/shard_map/all_gather | solution.py:182
  234.4 8.0 %fusion.27 = bf16[8,1,48,1024]{3,2,0,1:T(8,128)(2,1)S(1)} fusion(f32[8,48,1024]{2,1,0:T(8,128)S(1)} %fusion.6, bf16[8,48,4096]{2,1,0:T(8,128)(2,1)} %all-to-all-done, bf16[1,4096,1024]{2,1,0:T(8,128)(2,1)} %all-gather.9.cloned.1.call-done), kind=kOutput, calls=%fused_computation.43 | convolution fusion | flops 3223584768 | bytes 13893632 | tf_op jit(solution)/shard_map/sxcd,xdf->sxcf/dot_general | solution.py:186
  243.0 51.1 %all-gather.11.cloned.1.call-done = bf16[1,1024,4096]{2,1,0:T(8,128)(2,1)} async-done(((bf16[1,256,4096]{2,1,0:T(8,128)(2,1)}), bf16[1,1024,4096]{2,1,0:T(8,128)(2,1)}) %all-gather.11.cloned.1.call-update) | async-done | bytes 8388624 | tf_op jit(solution)/shard_map/all_gather | solution.py:183
  294.1 9.8 %convert_bitcast_fusion = bf16[4,8,1,48,4096]{4,3,1,0,2:T(8,128)(2,1)} fusion(bf16[4,256,4096,1]{2,1,3,0:T(8,128)(2,1)} %bitcast.166, bf16[8,48,4,256]{3,2,1,0:T(4,128)(2,1)S(1)} %reshape.413), kind=kOutput, calls=%fused_computation.6 | convolution fusion | flops 3227516928 | bytes 21757952 | tf_op jit(solution)/shard_map/sxcgf,xgfd->gsxcd/dot_general | solution.py:189
  303.9 9.7 %reduce_sum.70 = bf16[8,48,4096]{2,1,0:T(8,128)(2,1)} reduce(bf16[4,8,1,48,4096]{4,3,1,0,2:T(8,128)(2,1)} %convert_bitcast_fusion, bf16[]{:T(256)} %constant.105.clone.1), dimensions={0,2}, to_apply=%region_12.13 | reduce | flops 4718592 | bytes 15728642 | tf_op jit(solution)/shard_map/reduce_sum | solution.py:195
  313.6 5.6 %all-to-all-start.1 = ((bf16[8,1,48,4096]{3,2,1,0:T(8,128)(2,1)}), bf16[8,1,48,4096]{3,2,1,0:T(8,128)(2,1)S(1)}, u32[]{:S(2)}, u32[]{:S(2)}) async-start(bf16[8,1,48,4096]{3,2,1,0:T(8,128)(2,1)} %bitcast.163), calls=%async_computation.2 | async-start | bytes 6291456 | tf_op jit(solution)/shard_map/all_to_all | solution.py:196
  319.6 12.3 %convolution_convert_fusion = bf16[512,4096]{1,0:T(8,128)(2,1)} fusion(bf16[1024,4096]{1,0:T(8,128)(2,1)} %param.22, f32[512,1024]{1,0:T(8,128)} %bitcast.169, f32[512,1024]{1,0:T(8,128)} %copy.89, f32[512,1024]{1,0:T(8,128)} %copy.90, bf16[512,1024]{1,0:T(8,128)(2,1)} %param.19, f32[1024]{0:T(1024)S(1)} %copy-done.8), kind=kOutput, calls=%fused_computation.16 | convolution fusion | flops 4302307328 | bytes 19927040 | tf_op jit(solution)/shard_map/dot_general | solution.py:146
  331.9 58.5 %all-to-all-done.1 = bf16[8,1,48,4096]{3,2,1,0:T(8,128)(2,1)S(1)} async-done(((bf16[8,1,48,4096]{3,2,1,0:T(8,128)(2,1)}), bf16[8,1,48,4096]{3,2,1,0:T(8,128)(2,1)S(1)}, u32[]{:S(2)}, u32[]{:S(2)}) %all-to-all-start.1) | async-done | bytes 3145760 | tf_op jit(solution)/shard_map/all_to_all | solution.py:196
  392.6 3.8 all-to-all-start.2
  396.6 36.7 %all-to-all-done.2 = bf16[4,8,1,48,1024]{4,3,1,2,0:T(8,128)(2,1)S(1)} async-done(((bf16[4,8,1,48,1024]{4,3,1,2,0:T(8,128)(2,1)}), bf16[4,8,1,48,1024]{4,3,1,2,0:T(8,128)(2,1)S(1)}, u32[]{:S(2)}, u32[]{:S(2)}) %all-to-all-start.2) | async-done | bytes 3145760 | tf_op jit(solution)/shard_map/all_to_all | solution.py:198
  437.3 5.4 %gather_fusion.1 = bf16[1024,1024]{1,0:T(8,128)(2,1)} fusion(bf16[1536,1024]{1,0:T(8,128)(2,1)S(1)} %bitcast.159, s32[1024]{0:T(1024)S(1)} %broadcast_clamp_fusion), kind=kCustom, calls=%fused_computation.1 | custom fusion | bytes 4198400 | tf_op jit(solution)/shard_map/gather | solution.py:201
  442.7 5.4 %reshape.422 = f32[512,2,1024]{2,1,0:T(2,128)} reshape(bf16[1024,1024]{1,0:T(8,128)(2,1)} %gather_fusion.1) | data formatting | bytes 6291456 | tf_op jit(solution)/shard_map/convert_element_type | solution.py:201
  448.1 8.6 %multiply_reduce_fusion = bf16[512,1024]{1,0:T(8,128)(2,1)} fusion(f32[512,2,1024]{2,1,0:T(2,128)} %reshape.422, f32[512,2]{1,0:T(8,128)S(1)} %copy.100), kind=kLoop, calls=%fused_computation.17 | loop fusion | flops 1572864 | bytes 5246976 | tf_op jit(solution)/shard_map/reduce_sum | solution.py:202
  (118 shorter events, 52.3 us)
Async XLA Ops:
  7.2 141.4 %all-gather.13.cloned.1.call-start = ((), (), s32[]{:S(2)}) async-start(), calls=%async_computation.8 | async-start | bytes 2359296 | tf_op jit(solution)/shard_map/all_gather | solution.py:15
  9.5 4.2 copy-start.4
  18.2 4.1 copy-start.2
  25.5 2.1 copy-start.6
  25.5 147.9 %all-gather.7.cloned.1.call-start = ((), (), s32[]{:S(2)}) async-start(), calls=%async_computation.5 | async-start | bytes 10485760 | tf_op jit(solution)/shard_map/all_gather | solution.py:181
  26.3 208.1 %all-gather.9.cloned.1.call-start = ((), (), s32[]{:S(2)}) async-start(), calls=%async_computation.6 | async-start | bytes 10485760 | tf_op jit(solution)/shard_map/all_gather | solution.py:182
  27.0 267.1 %all-gather.11.cloned.1.call-start = ((), (), s32[]{:S(2)}) async-start(), calls=%async_computation.7 | async-start | bytes 10485760 | tf_op jit(solution)/shard_map/all_gather | solution.py:183
  27.6 12.1 %copy-start.5 = (f32[4096]{0:T(1024)S(1)}, f32[4096]{0:T(1024)}, u32[]{:S(2)}) copy-start(f32[4096]{0:T(1024)} %param.24) | copy-start | bytes 49156
  36.4 3.5 copy-start
  55.0 7.4 %copy-start.9 = (u32[32]{0:T(128)S(1)}, u32[32]{0:T(128)}, u32[]{:S(2)}) copy-start(u32[32]{0:T(128)} %constant.120) | copy-start | bytes 388
  55.0 116.7 %all-to-all-start = ((bf16[8,48,4096]{2,1,0:T(8,128)(2,1)}), bf16[8,48,4096]{2,1,0:T(8,128)(2,1)}, u32[]{:S(2)}, u32[]{:S(2)}) async-start(bf16[8,48,4096]{2,1,0:T(8,128)(2,1)} %bitcast.27), calls=%async_computation.1 | async-start | bytes 6291456 | tf_op jit(solution)/shard_map/all_to_all | solution.py:177
  138.6 5.4 %copy-start.3 = (bf16[512,1024]{1,0:T(8,128)(2,1)S(1)}, bf16[512,1024]{1,0:T(8,128)(2,1)}, u32[]{:S(2)}) copy-start(bf16[512,1024]{1,0:T(8,128)(2,1)} %param.18) | copy-start | bytes 3145732
  313.6 5.9 %copy-start.8 = (f32[1024]{0:T(1024)S(1)}, f32[1024]{0:T(1024)}, u32[]{:S(2)}) copy-start(f32[1024]{0:T(1024)} %param.21) | copy-start | bytes 12292
  313.6 76.8 %all-to-all-start.1 = ((bf16[8,1,48,4096]{3,2,1,0:T(8,128)(2,1)}), bf16[8,1,48,4096]{3,2,1,0:T(8,128)(2,1)S(1)}, u32[]{:S(2)}, u32[]{:S(2)}) async-start(bf16[8,1,48,4096]{3,2,1,0:T(8,128)(2,1)} %bitcast.163), calls=%async_computation.2 | async-start | bytes 6291456 | tf_op jit(solution)/shard_map/all_to_all | solution.py:196
  319.3 137.4 %reduce-scatter.2.cloned.1.call-start = ((), (), s32[]{:S(2)}) async-start(), calls=%async_computation.4 | async-start | bytes 5242880 | tf_op jit(solution)/shard_map/reduce_scatter | solution.py:145
  392.6 3.8 copy-start.7
  392.6 40.7 %all-to-all-start.2 = ((bf16[4,8,1,48,1024]{4,3,1,2,0:T(8,128)(2,1)}), bf16[4,8,1,48,1024]{4,3,1,2,0:T(8,128)(2,1)S(1)}, u32[]{:S(2)}, u32[]{:S(2)}) async-start(bf16[4,8,1,48,1024]{4,3,1,2,0:T(8,128)(2,1)} %pad_maximum_fusion), calls=%async_computation.3 | async-start | bytes 6291456 | tf_op jit(solution)/shard_map/all_to_all | solution.py:198
  433.3 1.7 copy-start.1
Sparse Core Ops, SparseCore 0:
  25.7 73.3 all-gather.12
  100.6 72.7 all-gather.6
  175.0 59.3 all-gather.8
  235.8 58.2 all-gather.10
  332.0 45.0 reduce-scatter.1
